TPU v7x, 32 devices: a whole 2x2x4 slice. The times are simulated.
32 devices in a mesh: sp: 4 (over z), tp: 4 (over y, x), dp: 2 (over core).
Axes of the slice: x: 2, y: 2, z: 4, core: 2. Of those that a mesh axis runs over, the one named last changes fastest.
Arguments:
- latents: bfloat16 [1024, 2048], P(('dp', 'sp', 'tp')), parts along dimension 0, may hold values from -6 to 6
- sample_vector: float32 [2, 2048], P('dp'), parts along dimension 0, may hold values from -6 to 6
- context: bfloat16 [512, 2048], P(('dp', 'sp')), parts along dimension 0, may hold values from -6 to 6
- context_vector: float32 [1, 2048], replicated, may hold values from -6 to 6
- norm_gain: float32 [2048], replicated, may hold values from 0.1 to 1.9
- modulator: bfloat16 [2048, 6144], P(None, ('sp', 'tp')), may hold values from -0.25 to 0.25
- query_weight: bfloat16 [2048, 1024], P('sp', 'tp'), may hold values from -0.125 to 0.125
- key_weight: bfloat16 [2048, 1024], P('sp', 'tp'), may hold values from -0.125 to 0.125
- value_weight: bfloat16 [2048, 2048], P('sp', 'tp'), may hold values from -0.125 to 0.125
- decay_down: bfloat16 [2048, 64], replicated, may hold values from -0.125 to 0.125
- decay_up: bfloat16 [2, 32, 1024], P(None, None, 'tp'), may hold values from -1 to 1
- decay_bias: float32 [2, 1024], P(None, 'tp'), as said below
- decay_extra: float32 [2, 1024, 8], P(None, ('dp', 'sp'), 'tp'), parts along dimension 1, may hold values from -2 to 0
- head_gain: float32 [256], replicated, may hold values from 0.1 to 1.9
- out_weight: bfloat16 [2048, 2048], P('tp'), may hold values from -0.125 to 0.125
Outputs:
- updated: bfloat16 [1024, 2048], P(('dp', 'sp', 'tp')), parts along dimension 0
There are 2 independent parts, one for each index of `dp`. A program takes and returns all parts, laid end to end along the dimension named above; an argument that names none is the same for every part. Nothing has to cross between parts.
Inputs may be any that keep to these rules, and one draw needn't show every extreme that they name: `decay_bias`: offsets of the decay gates,.
All inputs are finite; a program needn't handle non-finite values.
Results may differ from a plain program's by a relative error of at most 0.012.
Values may be sent and summed in bfloat16 or wider, within the bound.
A program may use at most 64 MiB of HBM per device.

v0:
```python
import jax
import jax.numpy as jnp
from jax import lax
from jax.sharding import PartitionSpec as P

DK = 128
DV = 256
RANK = 32
BLOCK = 64
CTX_LIFT = 4


epsilon = 1e-06
exponential_sharpness = 16.0
precise = lax.Precision.HIGHEST


def rms_rows(values, gains):
    values = values.astype(jnp.float32)
    return values * lax.rsqrt(jnp.mean(values * values, axis=-1, keepdims=True) + epsilon) * gains


def modulated(tokens, gains, modulation, model_width):
    shift_vector = modulation[:model_width]
    scale_vector = modulation[model_width : 2 * model_width]
    return (rms_rows(tokens, gains) * (1.0 + scale_vector) + shift_vector).astype(jnp.bfloat16)


def log_decays(low_rank, decay_up, decay_bias):
    fragment_sequence = []
    for direction in range(2):
        low_piece = lax.optimization_barrier(
            low_rank[:, direction * RANK : (direction + 1) * RANK]
        ).astype(jnp.float32)
        unnormalized_ratings = (
            jnp.dot(low_piece, decay_up[direction].astype(jnp.float32), precision=precise)
            + decay_bias[direction]
        )
        fragment_sequence.append(jax.nn.log_sigmoid(unnormalized_ratings) / exponential_sharpness)
    return jnp.stack(fragment_sequence)


def local_sweep(queries, key_rows, value_rows, decays, with_output):
    length = queries.shape[0]
    head_count = queries.shape[1]
    block_count = length // BLOCK

    def to_blocks(values):
        return values.reshape((block_count, BLOCK) + values.shape[1:])

    query_blocks = to_blocks(queries)
    key_blocks = to_blocks(key_rows)
    value_blocks = to_blocks(value_rows)
    within = jnp.cumsum(to_blocks(decays), axis=1)
    block_total = within[:, -1]
    update = jnp.einsum(
        "nshd,nshe->nhde",
        key_blocks * jnp.exp(block_total[:, None] - within),
        value_blocks,
        precision=precise,
    )

    def advance(carried, inputs):
        step_decay, step_update = inputs
        return (jnp.exp(step_decay)[:, :, None] * carried + step_update, carried)

    start_state = jnp.zeros((head_count, queries.shape[2], value_rows.shape[2]), jnp.float32)
    summary, previous = lax.scan(advance, start_state, (block_total, update))
    if not with_output:
        return summary
    device_decay = jnp.sum(block_total, axis=0)
    lower_mask = jnp.tril(jnp.ones((BLOCK, BLOCK), dtype=bool))
    query_dec = query_blocks * jnp.exp(within)
    scores = jnp.einsum(
        "nchd,nshd->nhcs", query_dec, key_blocks * jnp.exp(-within), precision=precise
    )
    scores = jnp.where(lower_mask[None, None], scores, 0.0)
    output = jnp.einsum("nhcs,nshe->nche", scores, value_blocks, precision=precise)
    output = output + jnp.einsum("nchd,nhde->nche", query_dec, previous, precision=precise)
    before = jnp.cumsum(block_total, axis=0) - block_total
    lifted = query_dec * jnp.exp(before)[:, None]
    return (
        output.reshape(length, head_count, -1),
        lifted.reshape(length, head_count, -1),
        device_decay,
        summary,
    )


def per_device(
    latents,
    sample_vector,
    context,
    context_vector,
    norm_gain,
    modulator,
    query_weight,
    key_weight,
    value_weight,
    decay_down,
    decay_up,
    decay_bias,
    decay_extra,
    head_gain,
    out_weight,
):
    model_width = latents.shape[1]
    conditions = jax.nn.silu(jnp.concatenate([sample_vector, context_vector], 0)).astype(
        jnp.bfloat16
    )
    local_mods = jnp.dot(conditions, modulator, preferred_element_type=jnp.float32)
    modulation = lax.all_gather(local_mods, ("sp", "tp"), axis=1, tiled=True)
    hidden = modulated(latents, norm_gain, modulation[0], model_width)
    context_hidden = modulated(context, norm_gain, modulation[1], model_width)
    token_rows = lax.all_gather(hidden, "tp", axis=0, tiled=True)
    row_count = token_rows.shape[0]
    joined = jnp.concatenate([token_rows, context_hidden], 0)
    head_count = decay_bias.shape[1] // DK
    query_sums = jnp.dot(
        joined[:row_count],
        lax.all_gather(query_weight, "sp", axis=0, tiled=True),
        preferred_element_type=jnp.float32,
    )
    key_sums = jnp.dot(
        joined,
        lax.all_gather(key_weight, "sp", axis=0, tiled=True),
        preferred_element_type=jnp.float32,
    )
    value_sums = jnp.dot(
        joined,
        lax.all_gather(value_weight, "sp", axis=0, tiled=True),
        preferred_element_type=jnp.float32,
    )
    low_rank = jnp.dot(joined, decay_down, preferred_element_type=jnp.float32).astype(jnp.bfloat16)
    key_all = key_sums.astype(jnp.bfloat16)
    value_all = value_sums.astype(jnp.bfloat16)
    context_keys, context_values, context_low = (
        lax.all_gather(key_all[row_count:], "sp", axis=0, tiled=True),
        lax.all_gather(value_all[row_count:], "sp", axis=0, tiled=True),
        lax.all_gather(low_rank[row_count:], "sp", axis=0, tiled=True),
    )

    def by_head(values, size):
        return (
            lax.optimization_barrier(values)
            .astype(jnp.float32)
            .reshape(values.shape[0], head_count, size)
        )

    queries = by_head(query_sums.astype(jnp.bfloat16), DK)
    key_rows = by_head(key_all[:row_count], DK)
    value_rows = by_head(value_all[:row_count], DV)
    context_key_rows = by_head(context_keys, DK)
    context_value_rows = by_head(context_values, DV)
    decays = (
        log_decays(low_rank[:row_count], decay_up, decay_bias).reshape(2, row_count, head_count, DK)
        + decay_extra[:, :, :, None]
    )
    context_decays = log_decays(context_low, decay_up, decay_bias).reshape(
        2, context_low.shape[0], head_count, DK
    )
    forward_out, forward_lift, forward_decay, forward_state = local_sweep(
        queries, key_rows, value_rows, decays[0], True
    )
    backward_out, backward_lift, backward_decay, backward_state = local_sweep(
        queries[::-1], key_rows[::-1], value_rows[::-1], decays[1][::-1], True
    )
    context_forward = CTX_LIFT * local_sweep(
        context_key_rows, context_key_rows, context_value_rows, context_decays[0], False
    )
    context_backward = CTX_LIFT * local_sweep(
        context_key_rows[::-1],
        context_key_rows[::-1],
        context_value_rows[::-1],
        context_decays[1][::-1],
        False,
    )
    decays_all, states_all = (
        lax.all_gather(
            jnp.stack([forward_decay, backward_decay])[None].astype(jnp.bfloat16),
            "sp",
            axis=0,
            tiled=True,
        ).astype(jnp.float32),
        lax.all_gather(
            jnp.stack([forward_state, backward_state])[None].astype(jnp.bfloat16),
            "sp",
            axis=0,
            tiled=True,
        ).astype(jnp.float32),
    )
    my_index = lax.axis_index("sp")
    device_count = lax.axis_size("sp")

    def fold_step(turn_index, carries):
        forward_in, backward_in = carries
        back_index = device_count - 1 - turn_index
        moved_forward = (
            jnp.exp(decays_all[turn_index, 0])[:, :, None] * forward_in + states_all[turn_index, 0]
        )
        moved_backward = (
            jnp.exp(decays_all[back_index, 1])[:, :, None] * backward_in + states_all[back_index, 1]
        )
        forward_in = jnp.where(turn_index < my_index, moved_forward, forward_in)
        backward_in = jnp.where(back_index > my_index, moved_backward, backward_in)
        return (forward_in, backward_in)

    forward_in, backward_in = lax.fori_loop(
        0, device_count, fold_step, (context_forward, context_backward)
    )
    forward = forward_out + jnp.einsum("lhd,hde->lhe", forward_lift, forward_in, precision=precise)
    backward = backward_out + jnp.einsum(
        "lhd,hde->lhe", backward_lift, backward_in, precision=precise
    )
    mixed = forward + backward[::-1]
    normed = rms_rows(mixed, head_gain).astype(jnp.bfloat16).reshape(row_count, head_count * DV)
    summed = lax.psum_scatter(
        jnp.dot(normed, out_weight, preferred_element_type=jnp.float32).astype(jnp.bfloat16),
        "tp",
        scatter_dimension=0,
        tiled=True,
    )
    projected = lax.optimization_barrier(summed).astype(jnp.float32)
    gate_vector = modulation[0, 2 * model_width :]
    return (latents.astype(jnp.float32) + gate_vector * projected).astype(jnp.bfloat16)


def solution(mesh):
    placed = (
        P(("dp", "sp", "tp"), None),
        P("dp", None),
        P(("dp", "sp"), None),
        P(),
        P(),
        P(None, ("sp", "tp")),
        P("sp", "tp"),
        P("sp", "tp"),
        P("sp", "tp"),
        P(),
        P(None, None, "tp"),
        P(None, "tp"),
        P(None, ("dp", "sp"), "tp"),
        P(),
        P("tp", None),
    )
    return jax.shard_map(
        per_device,
        mesh=mesh,
        in_specs=placed,
        out_specs=P(("dp", "sp", "tp"), None),
        check_vma=False,
    )
```

profile of v0, /device:TPU:0, one launch (start us, length us, event | category | flops | bytes accessed | tf_op | source)
XLA Modules:
  0.0 275.8 jit_solution(16105974951668865694)
XLA Ops:
  10.6 43.3 %all_gather.30 = f32[2,6144]{1,0:T(2,128)S(1)} all-gather(f32[2,384]{1,0:T(2,128)S(1)} %fusion.65), channel_id=1, replica_groups=mesh['sp'=4,'tp'=4,'dp'=2] {'sp','tp'}, dimensions={1}, use_global_device_ids=true | all-gather | bytes 52224 | tf_op jit(solution)/shard_map/all_gather | solution.py:112
  55.0 8.5 %all_gather.31 = bf16[128,2048]{1,0:T(8,128)(2,1)S(1)} all-gather(bf16[32,2048]{1,0:T(8,128)(2,1)S(1)} %fusion.26), channel_id=1, replica_groups=mesh['sp'=4,'tp'=4,'dp'=2] {'tp'}, dimensions={0}, use_global_device_ids=true | all-gather | bytes 655360 | tf_op jit(solution)/shard_map/all_gather | solution.py:115
  72.4 13.7 %all_gather.35 = bf16[256,64]{1,0:T(8,128)(2,1)S(1)} all-gather(bf16[64,64]{1,0:T(8,128)(2,1)S(1)} %copy.74), channel_id=1, replica_groups=mesh['sp'=4,'tp'=4,'dp'=2] {'sp'}, dimensions={0}, use_global_device_ids=true | all-gather | bytes 40960 | tf_op jit(solution)/shard_map/all_gather | solution.py:140
  89.7 1.9 fusion.29
  94.0 8.0 %all_gather.38 = bf16[4,2,2,128]{3,2,1,0:T(2,128)(2,1)S(1)} all-gather(bf16[1,2,2,128]{3,2,1,0:T(2,128)(2,1)S(1)} %pad_maximum_fusion.6), channel_id=1, replica_groups=mesh['sp'=4,'tp'=4,'dp'=2] {'sp'}, dimensions={0}, use_global_device_ids=true | all-gather | bytes 5120 | tf_op jit(solution)/shard_map/all_gather | solution.py:179
  108.2 14.1 %all_gather.36 = bf16[256,256]{1,0:T(8,128)(2,1)S(1)} all-gather(bf16[64,256]{1,0:T(8,128)(2,1)S(1)} %slice.131), channel_id=1, replica_groups=mesh['sp'=4,'tp'=4,'dp'=2] {'sp'}, dimensions={0}, use_global_device_ids=true | all-gather | bytes 163840 | tf_op jit(solution)/shard_map/all_gather | solution.py:138
  133.5 1.9 fusion.77
  136.8 1.9 fusion.76
  143.8 2.4 convolution_convert_fusion.1
  146.9 13.8 %all_gather.37 = bf16[256,512]{1,0:T(8,128)(2,1)S(1)} all-gather(bf16[64,512]{1,0:T(8,128)(2,1)S(1)} %slice.132), channel_id=1, replica_groups=mesh['sp'=4,'tp'=4,'dp'=2] {'sp'}, dimensions={0}, use_global_device_ids=true | all-gather | bytes 327680 | tf_op jit(solution)/shard_map/all_gather | solution.py:139
  167.3 2.0 fusion.36
  169.3 2.3 fusion.38
  172.5 3.6 %while.69 = (s32[]{:T(128)}, f32[2,128,256]{2,1,0:T(8,128)S(1)}, f32[2,2,128,256]{3,2,1,0:T(8,128)}, f32[2,2,128]{2,1,0:T(2,128)S(1)}, f32[2,2,128,256]{3,2,1,0:T(8,128)}, /*index=5*/s32[]{:T(128)}, s32[]{:T(128)}) while((s32[]{:T(128)}, f32[2,128,256]{2,1,0:T(8,128)S(1)}, f32[2,2,128,256]{3,2,1,0:T(8,128)}, ...), condition=%wide.region_15.16_spmd.clone, body=%wide.region_14.15_spmd.clone.sunk | while | flops 262147 | bytes 1313900 | solution.py:68
  180.2 1.9 copy.149
  182.1 4.7 %rev.26 = f32[256,2,256]{2,0,1:T(8,128)} reverse(f32[256,2,256]{2,0,1:T(8,128)} %bitcast.172), dimensions={0} | reverse | bytes 1048576 | tf_op jit(solution)/shard_map/rev | solution.py:174
  186.8 3.1 %fusion.20 = f32[4,2,128,256]{3,2,1,0:T(8,128)} fusion(f32[4,64,2,256]{3,1,0,2:T(8,128)} %bitcast.170, f32[4,64,2,128]{3,2,1,0:T(2,128)S(1)} %copy-done.12), kind=kOutput, calls=%fused_computation.59 | convolution fusion | flops 201326592 | bytes 1835008 | tf_op jit(solution)/shard_map/nshd,nshe->nhde/dot_general | solution.py:56
  189.9 4.5 %while.68 = (s32[]{:T(128)}, f32[2,128,256]{2,1,0:T(8,128)S(1)}, f32[4,2,128]{2,1,0:T(2,128)S(1)}, f32[4,2,128,256]{3,2,1,0:T(8,128)}, s32[]{:T(128)}, /*index=5*/s32[]{:T(128)}) while((s32[]{:T(128)}, f32[2,128,256]{2,1,0:T(8,128)S(1)}, f32[4,2,128]{2,1,0:T(2,128)S(1)}, f32[4,2,128,256]{3,2,1,0:T(8,128)}, s32[]{:T(128)}, ...), condition=%wide.region_10.11_spmd.clone, body=%wide.region_9.10_spmd.clone.sunk | while | flops 196611 | bytes 789599 | solution.py:68
  196.5 3.7 %while.66 = (s32[]{:T(128)}, f32[2,128,256]{2,1,0:T(8,128)S(1)}, f32[2,2,128,256]{3,2,1,0:T(8,128)}, f32[2,2,128]{2,1,0:T(2,128)S(1)}, f32[2,2,128,256]{3,2,1,0:T(8,128)}, /*index=5*/s32[]{:T(128)}, s32[]{:T(128)}) while((s32[]{:T(128)}, f32[2,128,256]{2,1,0:T(8,128)S(1)}, f32[2,2,128,256]{3,2,1,0:T(8,128)}, ...), condition=%wide.region_4.5_spmd.clone, body=%wide.region_3.4_spmd.clone.sunk | while | flops 262147 | bytes 1313900 | solution.py:68
  202.8 2.6 fusion.33
  205.3 4.4 %while.67 = (s32[]{:T(128)}, f32[2,128,256]{2,1,0:T(8,128)S(1)}, f32[4,2,128]{2,1,0:T(2,128)S(1)}, f32[4,2,128,256]{3,2,1,0:T(8,128)}, s32[]{:T(128)}, /*index=5*/s32[]{:T(128)}) while((s32[]{:T(128)}, f32[2,128,256]{2,1,0:T(8,128)S(1)}, f32[4,2,128]{2,1,0:T(2,128)S(1)}, f32[4,2,128,256]{3,2,1,0:T(8,128)}, s32[]{:T(128)}, ...), condition=%wide.region_7.8_spmd.clone, body=%wide.region_6.7_spmd.clone.sunk | while | flops 196611 | bytes 789599 | solution.py:68
  209.8 18.7 %all-gather.11.cloned.1.call-done = bf16[4,2,2,128,256]{4,3,2,1,0:T(8,128)(2,1)} async-done(((bf16[1,2,2,128,256]{4,3,2,1,0:T(8,128)(2,1)}), bf16[4,2,2,128,256]{4,3,2,1,0:T(8,128)(2,1)}) %all-gather.11.cloned.1.call-update) | async-done | bytes 1048592 | tf_op jit(solution)/shard_map/all_gather | solution.py:185
  228.5 2.8 %convert_element_type.96 = f32[4,2,2,128,256]{4,3,2,1,0:T(8,128)} convert(bf16[4,2,2,128,256]{4,3,2,1,0:T(8,128)(2,1)} %all-gather.11.cloned.1.call-done) | non-fusion elementwise | flops 524288 | bytes 3145728 | tf_op jit(solution)/shard_map/convert_element_type | solution.py:190
  231.3 7.8 %while.65 = (s32[]{:T(128)}, f32[2,128,256]{2,1,0:T(8,128)S(1)}, f32[2,128,256]{2,1,0:T(8,128)S(1)}, s32[]{:T(128)}, f32[4,2,2,128]{3,2,1,0:T(2,128)}, /*index=5...) while((s32[]{:T(128)}, f32[2,128,256]{2,1,0:T(8,128)S(1)}, ...), condition=%wide.region_17.18_spmd, body=%wide.region_16.17_spmd.sunk | while | flops 393224 | bytes 1579199 | solution.py:208
  243.1 24.6 %reduce-scatter.2.cloned.1.call-done = bf16[32,2048]{1,0:T(8,128)(2,1)} async-done(((bf16[128,2048]{1,0:T(8,128)(2,1)}), bf16[32,2048]{1,0:T(8,128)(2,1)}) %reduce-scatter.2.cloned.1.call-update) | async-done | bytes 131088 | tf_op jit(solution)/shard_map/reduce_scatter | solution.py:217
  (212 shorter events, 89.6 us)
Async XLA Ops:
  6.5 235.2 %copy-start = (bf16[512,2048]{1,0:T(8,128)(2,1)S(1)}, bf16[512,2048]{1,0:T(8,128)(2,1)}, u32[]{:S(2)}) copy-start(bf16[512,2048]{1,0:T(8,128)(2,1)} %param.39) | copy-start | bytes 6291460
  6.5 48.0 %copy-start.18 = (bf16[64,2048]{1,0:T(8,128)(2,1)S(1)}, bf16[64,2048]{1,0:T(8,128)(2,1)}, u32[]{:S(2)}) copy-start(bf16[64,2048]{1,0:T(8,128)(2,1)} %param.27) | copy-start | bytes 786436
  6.5 48.2 %copy-start.5 = (bf16[32,2048]{1,0:T(8,128)(2,1)S(1)}, bf16[32,2048]{1,0:T(8,128)(2,1)}, u32[]{:S(2)}) copy-start(bf16[32,2048]{1,0:T(8,128)(2,1)} %param.25) | copy-start | bytes 393220
  6.5 48.4 %copy-start.28 = (f32[2048]{0:T(1024)S(1)}, f32[2048]{0:T(1024)}, u32[]{:S(2)}) copy-start(f32[2048]{0:T(1024)} %param.29) | copy-start | bytes 24580
  6.5 99.8 %all-gather.9.cloned.1.call-start = ((), (), s32[]{:S(2)}) async-start(), calls=%async_computation.3 | async-start | bytes 1310720 | tf_op jit(solution)/shard_map/all_gather | solution.py:126
  7.3 118.1 %all-gather.7.cloned.1.call-start = ((), (), s32[]{:S(2)}) async-start(), calls=%async_computation.2 | async-start | bytes 1310720 | tf_op jit(solution)/shard_map/all_gather | solution.py:121
  8.0 135.8 %all-gather.5.cloned.1.call-start = ((), (), s32[]{:S(2)}) async-start(), calls=%async_computation.1 | async-start | bytes 2621440 | tf_op jit(solution)/shard_map/all_gather | solution.py:131
  8.8 219.7 %all-gather.11.cloned.1.call-start = ((), (), s32[]{:S(2)}) async-start(), calls=%async_computation.4 | async-start | bytes 1310720 | tf_op jit(solution)/shard_map/all_gather | solution.py:185
  8.8 55.5 %copy-start.33 = (bf16[2048,64]{0,1:T(8,128)(2,1)S(1)}, bf16[2048,64]{0,1:T(8,128)(2,1)}, u32[]{:S(2)}) copy-start(bf16[2048,64]{0,1:T(8,128)(2,1)} %param.34) | copy-start | bytes 786436
  54.9 10.5 %copy-start.30 = (f32[2,256]{1,0:T(2,128)S(1)}, f32[2,256]{1,0:T(2,128)}, u32[]{:S(2)}) copy-start(f32[2,256]{1,0:T(2,128)} %param.36) | copy-start | bytes 6148
  54.9 11.6 %copy-start.34 = (bf16[2,32,256]{2,1,0:T(8,128)(2,1)S(1)}, bf16[2,32,256]{2,1,0:T(8,128)(2,1)}, u32[]{:S(2)}) copy-start(bf16[2,32,256]{2,1,0:T(8,128)(2,1)} %param.35) | copy-start | bytes 98308
  133.5 8.6 %copy-start.9 = (f32[4,64,2,128]{3,2,1,0:T(2,128)S(1)}, f32[4,64,2,128]{3,2,1,0:T(2,128)}, u32[]{:S(2)}) copy-start(f32[4,64,2,128]{3,2,1,0:T(2,128)} %copy-done.8) | copy-start | bytes 786436
  133.5 8.6 %copy-start.17 = (f32[256,2,128]{2,1,0:T(2,128)S(1)}, f32[256,2,128]{2,1,0:T(2,128)}, u32[]{:S(2)}) copy-start(f32[256,2,128]{2,1,0:T(2,128)} %rev.25) | copy-start | bytes 786436
  135.4 7.5 %copy-start.3 = (f32[2,64,2,128]{3,2,1,0:T(2,128)}, f32[2,64,2,128]{3,2,1,0:T(2,128)S(1)}, u32[]{:S(2)}) copy-start(f32[2,64,2,128]{3,2,1,0:T(2,128)S(1)} %get-tuple-element.397) | copy-start | bytes 393220
  135.4 7.5 %copy-start.11 = (f32[4,64,2,128]{3,2,1,0:T(2,128)S(1)}, f32[4,64,2,128]{3,2,1,0:T(2,128)}, u32[]{:S(2)}) copy-start(f32[4,64,2,128]{3,2,1,0:T(2,128)} %copy-done.10) | copy-start | bytes 786436
  135.4 7.5 %copy-start.16 = (f32[4,64,2,128]{3,2,1,0:T(2,128)S(1)}, f32[4,64,2,128]{3,2,1,0:T(2,128)}, u32[]{:S(2)}) copy-start(f32[4,64,2,128]{3,2,1,0:T(2,128)} %reshape_reshape.20) | copy-start | bytes 786436
  164.9 7.6 %copy-start.27 = (f32[2,2,128]{2,1,0:T(2,128)S(1)}, f32[2,2,128]{2,1,0:T(2,128)}, u32[]{:S(2)}) copy-start(f32[2,2,128]{2,1,0:T(2,128)} %get-tuple-element.581) | copy-start | bytes 6148
  177.6 9.2 %copy-start.12 = (f32[4,64,2,128]{3,2,1,0:T(2,128)S(1)}, f32[4,64,2,128]{3,2,1,0:T(2,128)}, u32[]{:S(2)}) copy-start(f32[4,64,2,128]{3,2,1,0:T(2,128)} %exponential_multiply_fusion) | copy-start | bytes 786436
  189.9 6.6 %copy-start.26 = (f32[2,2,128]{2,1,0:T(2,128)S(1)}, f32[2,2,128]{2,1,0:T(2,128)}, u32[]{:S(2)}) copy-start(f32[2,2,128]{2,1,0:T(2,128)} %get-tuple-element.638) | copy-start | bytes 6148
  200.9 66.8 %reduce-scatter.2.cloned.1.call-start = ((), (), s32[]{:S(2)}) async-start(), calls=%async_computation.5 | async-start | bytes 655360 | tf_op jit(solution)/shard_map/reduce_scatter | solution.py:217
  231.3 7.8 %copy-start.15 = (f32[128,2,256]{0,2,1:T(8,128)S(1)}, f32[128,2,256]{0,2,1:T(8,128)}, u32[]{:S(2)}) copy-start(f32[128,2,256]{0,2,1:T(8,128)} %copy.99) | copy-start | bytes 786436
  231.3 7.8 %copy-start.22 = (f32[128,2,128]{2,0,1:T(8,128)S(1)}, f32[128,2,128]{2,0,1:T(8,128)}, u32[]{:S(2)}) copy-start(f32[128,2,128]{2,0,1:T(8,128)} %bitcast_multiply_fusion) | copy-start | bytes 393220
  241.8 25.9 %copy-start.6 = (bf16[32,2048]{1,0:T(8,128)(2,1)S(1)}, bf16[32,2048]{1,0:T(8,128)(2,1)}, u32[]{:S(2)}) copy-start(bf16[32,2048]{1,0:T(8,128)(2,1)} %param.25) | copy-start | bytes 393220
  241.8 25.9 %copy-start.29 = (f32[1,2048]{1,0:T(1,128)S(1)}, f32[1,2048]{1,0:T(1,128)}, u32[]{:S(2)}) copy-start(f32[1,2048]{1,0:T(1,128)} %get-tuple-element.406) | copy-start | bytes 24580
  (16 other events, 36.4 us)
Sparse Core Ops, SparseCore 0:
  8.9 30.9 all-gather.8
  41.5 27.5 all-gather.6
  70.7 46.9 all-gather.4
  201.1 27.3 all-gather.10
  243.2 24.4 reduce-scatter.1
where the time goes:
time: 278 us; the launch traced here: 276 us
  blocking collectives  101 us (36%)
  waiting for transfers between devices  45.4 us (16%)
  other arithmetic  43.1 us (16%)
  local copies, waits for them, and re-layouts  40.5 us (15%)
  matrix products  31 us (11%)
  between operations  13.7 us (5%)
    all_gather x1, blocking collectives, per_device(): modulation = lax.all_gather(local_mods, ('sp', 'tp'), axis=1, tiled=True)  43.3 us
    reduce_scatter x1, waiting for transfers between devices, per_device(): lax.psum_scatter(jnp.dot(normed, out_weight, preferred_element_type=jnp.f...  24.6 us
    all_gather x1, waiting for transfers between devices, per_device(): lax.all_gather(jnp.stack([forward_state, backward_state])[None].astype(jn...  18.7 us
    all_gather x1, blocking collectives, per_device(): lax.all_gather(key_all[row_count:], 'sp', axis=0, tiled=True)  14.1 us
    all_gather x1, blocking collectives, per_device(): lax.all_gather(value_all[row_count:], 'sp', axis=0, tiled=True)  13.8 us
    all_gather x1, blocking collectives, per_device(): lax.all_gather(low_rank[row_count:], 'sp', axis=0, tiled=True)  13.7 us
    add x12, other arithmetic, advance(): return (jnp.exp(step_decay)[:, :, None] * carried + step_update, carried)  12.9 us
    dot_general x4, matrix products, local_sweep(): jnp.einsum('nshd,nshe->nhde', key_blocks * jnp.exp(block_total[:, None] -...  9.18 us
  transfers between devices with their start and end apart: 5, of which 2 were waited for; matrix products, arithmetic and copies ran while one was open for 19% of the time, Pallas kernels for 0%

commit v1 on v0

v1 whole, which is shorter than its diff:
```python
import functools

import jax
import jax.numpy as jnp
from jax import lax
from jax.experimental import pallas as pl
from jax.experimental.pallas import tpu as pltpu
from jax.sharding import PartitionSpec as P

DK = 128
BLOCK = 64
CTX_LIFT = 4
EPS = 1e-06
SHARP = 16.0
F32 = jnp.float32
BF16 = jnp.bfloat16
MESH = pl.DeviceIdType.MESH
HIGH = lax.Precision.HIGHEST


def dot(a, b):
    return jnp.dot(a, b, preferred_element_type=F32)


def dot_nt(a, b):
    return lax.dot_general(a, b, (((1,), (1,)), ((), ())), preferred_element_type=F32)


def dot_tn(a, b):
    return lax.dot_general(a, b, (((0,), (0,)), ((), ())), preferred_element_type=F32)


def sums(mask, values):
    return jnp.dot(mask.astype(F32), values, precision=HIGH, preferred_element_type=F32)


def log_sigmoid(x):
    return jnp.minimum(x, 0.0) - jnp.log1p(jnp.exp(-jnp.abs(x)))


def kernel(
    n_sp,
    n_tp,
    latents,
    sample_vector,
    context,
    context_vector,
    norm_gain,
    modulator,
    query_weight,
    key_weight,
    value_weight,
    decay_down,
    decay_up,
    decay_bias,
    decay_extra,
    head_gain,
    out_weight,
    out,
    mod_w,
    mods,
    lat,
    hid,
    wk,
    wv,
    wq,
    wo,
    acc_k,
    acc_v,
    acc_q,
    c_low,
    c_key,
    c_val,
    st_own,
    st_all,
    tot_own,
    tot_all,
    fold,
    normed,
    part,
    rs,
    loc_sem,
    mod_s,
    mod_r,
    lat_s,
    lat_r,
    w_s,
    w_r,
    p_s,
    p_r,
    cx_s,
    cx_r,
    st_s,
    st_r,
    rs_s,
    rs_r,
):
    s = lax.axis_index("sp")
    t = lax.axis_index("tp")
    d = lax.axis_index("dp")
    h = lax.rem(d, 2)
    mate = d + 1 - 2 * h
    n_dev = n_sp * n_tp
    me = s * n_tp + t
    rows, width = latents.shape
    ctx_rows = context.shape[0]
    length = rows * n_tp
    total = length + ctx_rows
    depth = hid.shape[2]
    half = depth // 2
    heads = decay_bias.shape[1] // DK
    dv = head_gain.shape[1]
    rank = decay_up.shape[1]

    def peer(k):
        other = lax.rem(me + k, n_dev)
        return {"sp": other // n_tp, "tp": lax.rem(other, n_tp)}

    weights = ((key_weight, wk), (value_weight, wv), (query_weight, wq))
    local = [pltpu.make_async_copy(modulator, mod_w, loc_sem.at[0])]
    for m, (source, slots) in enumerate(weights):
        for i in range(2):
            local.append(
                pltpu.make_async_copy(
                    source.at[pl.ds(i * half, half)], slots.at[s, i], loc_sem.at[1 + 2 * m + i]
                )
            )
    local.append(pltpu.make_async_copy(out_weight, wo, loc_sem.at[7]))
    for copy in local:
        copy.start()

    barrier = pltpu.get_barrier_semaphore()
    for k in range(1, n_dev):
        pl.semaphore_signal(barrier, inc=1, device_id=peer(k), device_id_type=MESH)
    pl.semaphore_signal(barrier, inc=1, device_id={"dp": mate}, device_id_type=MESH)
    pl.semaphore_wait(barrier, n_dev)

    def ring_copy(m, r, j, first=False):
        source, slots = weights[m]
        origin = s - j if r == 0 else s + j
        target = s + 1 if r == 0 else s - 1
        src = source.at[pl.ds(h * half, half)] if first else slots.at[origin, h]
        return pltpu.make_async_remote_copy(
            src_ref=src,
            dst_ref=slots.at[origin, h],
            send_sem=w_s.at[m, r, j],
            recv_sem=w_r.at[m, r, j],
            device_id={"sp": target},
            device_id_type=MESH,
        )

    def ring_arrival(m, r, j):
        slots = weights[m][1]
        origin = s - j if r == 0 else s + j
        return pltpu.make_async_remote_copy(
            src_ref=slots.at[origin, h],
            dst_ref=slots.at[origin, h],
            send_sem=w_s.at[m, r, j - 1],
            recv_sem=w_r.at[m, r, j - 1],
            device_id={"sp": s},
            device_id_type=MESH,
        )

    def mate_copy(m, r, j, side):
        slots = weights[m][1]
        origin = s - j if r == 0 else s + j
        return pltpu.make_async_remote_copy(
            src_ref=slots.at[origin, side],
            dst_ref=slots.at[origin, side],
            send_sem=p_s.at[m, r, j - 1],
            recv_sem=p_r.at[m, r, j - 1],
            device_id={"dp": mate},
            device_id_type=MESH,
        )

    def exists(r, j):
        return s - j >= 0 if r == 0 else s + j < n_sp

    def onward(r):
        return s + 1 < n_sp if r == 0 else s - 1 >= 0

    def send_own(m):
        for r in range(2):

            @pl.when(onward(r))
            def _():
                ring_copy(m, r, 0, True).start()

    def relay(m, j):
        for r in range(2):

            @pl.when(exists(r, j))
            def _():
                ring_arrival(m, r, j).wait_recv()
                if j < n_sp - 1:

                    @pl.when(onward(r))
                    def _():
                        ring_copy(m, r, j).start()

                mate_copy(m, r, j, h).start()

    def whole(slots, o):
        return slots[o].reshape(depth, slots.shape[3])

    def multiply(m, j, acc, count):
        slots = weights[m][1]
        for r in range(2):

            @pl.when(exists(r, j))
            def _():
                origin = s - j if r == 0 else s + j
                mate_copy(m, r, j, 1 - h).wait_recv()
                acc[...] += dot(hid[origin, 0:count], whole(slots, origin))

    lat_copies = []
    for k in range(1, n_tp):
        lat_copies.append(
            pltpu.make_async_remote_copy(
                src_ref=latents,
                dst_ref=lat.at[t],
                send_sem=lat_s.at[k],
                recv_sem=lat_r.at[k],
                device_id={"tp": lax.rem(t + k, n_tp)},
                device_id_type=MESH,
            )
        )
    send_own(0)
    send_own(1)
    for copy in lat_copies:
        copy.start()

    is_first = lax.broadcasted_iota(jnp.int32, (16, width), 0) == 0
    vectors = jnp.where(is_first, sample_vector[...], context_vector[...])
    conditions = (vectors / (1.0 + jnp.exp(-vectors))).astype(BF16)
    local[0].wait()
    mods[me] = dot(conditions, mod_w[...])[0:8]
    mod_copies = []
    for k in range(1, n_dev):
        copy = pltpu.make_async_remote_copy(
            src_ref=mods.at[me],
            dst_ref=mods.at[me],
            send_sem=mod_s.at[k],
            recv_sem=mod_r.at[k],
            device_id=peer(k),
            device_id_type=MESH,
        )
        copy.start()
        mod_copies.append(copy)

    lat[t] = latents[...]
    for k in range(1, n_tp):
        pltpu.make_async_remote_copy(
            src_ref=latents,
            dst_ref=lat.at[lax.rem(t - k + n_tp, n_tp)],
            send_sem=lat_s.at[k],
            recv_sem=lat_r.at[k],
            device_id={"tp": t},
            device_id_type=MESH,
        ).wait_recv()
    for k in range(1, n_dev):
        other = lax.rem(me - k + n_dev, n_dev)
        pltpu.make_async_remote_copy(
            src_ref=mods.at[me],
            dst_ref=mods.at[other],
            send_sem=mod_s.at[k],
            recv_sem=mod_r.at[k],
            device_id={"tp": t},
            device_id_type=MESH,
        ).wait_recv()
    modulation = jnp.concatenate([mods[i] for i in range(n_dev)], axis=1)
    gate = modulation[0:1, 2 * width :]

    def modulated(x, row):
        x = x.astype(F32)
        x = x * lax.rsqrt(jnp.mean(x * x, axis=-1, keepdims=True) + EPS) * norm_gain[...]
        shift = modulation[row : row + 1, :width]
        scale = modulation[row : row + 1, width : 2 * width]
        return (x * (1.0 + scale) + shift).astype(BF16)

    def put(x, at):
        count = x.shape[0]
        for o in range(n_sp):
            hid[o, at : at + count] = x[:, o * depth : (o + 1) * depth]

    for i in range(n_tp):
        put(modulated(lat[i], 0), i * rows)
    piece = min(32, ctx_rows)
    for i in range(ctx_rows // piece):
        put(modulated(context[i * piece : (i + 1) * piece], 1), length + i * piece)

    low = dot(hid[0], decay_down[0:depth])
    for o in range(1, n_sp):
        low = low + dot(hid[o], decay_down[o * depth : (o + 1) * depth])
    low = low.astype(BF16)

    def ctx_copy(i, buffer, k):
        other = lax.rem(s + k, n_sp)
        return pltpu.make_async_remote_copy(
            src_ref=buffer.at[s],
            dst_ref=buffer.at[s],
            send_sem=cx_s.at[i, k],
            recv_sem=cx_r.at[i, k],
            device_id={"sp": other},
            device_id_type=MESH,
        )

    def ctx_arrival(i, buffer, k):
        other = lax.rem(s - k + n_sp, n_sp)
        return pltpu.make_async_remote_copy(
            src_ref=buffer.at[s],
            dst_ref=buffer.at[other],
            send_sem=cx_s.at[i, k],
            recv_sem=cx_r.at[i, k],
            device_id={"sp": s},
            device_id_type=MESH,
        )

    c_low[s] = low[length:]
    for k in range(1, n_sp):
        ctx_copy(0, c_low, k).start()

    def log_decays(values, z):
        x = dot(values[:, z * rank : (z + 1) * rank], decay_up[z]) + decay_bias[z : z + 1]
        return log_sigmoid(x) / SHARP

    def wide(z):
        extra = decay_extra[z]
        return jnp.concatenate(
            [jnp.broadcast_to(extra[:, g : g + 1], (length, DK)) for g in range(heads)], axis=1
        )

    row_id = lax.broadcasted_iota(jnp.int32, (length, length), 0)
    col_id = lax.broadcasted_iota(jnp.int32, (length, length), 1)
    same = row_id // BLOCK == col_id // BLOCK
    within = [
        sums(same & (col_id <= row_id), log_decays(low[:length], 0) + wide(0)),
        sums(same & (col_id >= row_id), log_decays(low[:length], 1) + wide(1)),
    ]
    blocks = length // BLOCK
    totals = [
        [within[0][(b + 1) * BLOCK - 1 : (b + 1) * BLOCK] for b in range(blocks)],
        [within[1][b * BLOCK : b * BLOCK + 1] for b in range(blocks)],
    ]
    none = jnp.zeros_like(totals[0][0])

    def between(z, lo, hi):
        value = none
        for b in range(lo, hi):
            value = value + totals[z][b]
        return value

    tot_own[...] = jnp.concatenate(
        [between(0, 0, blocks), between(1, 0, blocks)] + [none] * 6, axis=0
    )

    for k in range(1, n_sp):
        ctx_arrival(0, c_low, k).wait_recv()
    lows = jnp.concatenate([c_low[o] for o in range(n_sp)], axis=0)
    ctx_all = n_sp * ctx_rows
    crow = lax.broadcasted_iota(jnp.int32, (ctx_all, ctx_all), 0)
    ccol = lax.broadcasted_iota(jnp.int32, (ctx_all, ctx_all), 1)
    ctx_weight = [
        jnp.exp(sums(ccol > crow, log_decays(lows, 0))),
        jnp.exp(sums(ccol < crow, log_decays(lows, 1))),
    ]

    for copy in local[1:5]:
        copy.wait()
    acc_k[...] = dot(hid[s], whole(wk, s))
    acc_v[...] = dot(hid[s], whole(wv, s))
    for j in range(1, n_sp):
        relay(0, j)
        relay(1, j)
        if j == n_sp - 1:
            send_own(2)
        multiply(0, j, acc_k, total)
        multiply(1, j, acc_v, total)
    keys = acc_k[...].astype(BF16)
    values = acc_v[...].astype(BF16)
    c_key[s] = keys[length:]
    c_val[s] = values[length:]
    for k in range(1, n_sp):
        ctx_copy(1, c_key, k).start()
        ctx_copy(2, c_val, k).start()
    keys = keys[:length].astype(F32)
    values = values[:length]

    def per_block(f):
        return jnp.concatenate([f(b) for b in range(blocks)], axis=0)

    def rows_of(x, b):
        return x[b * BLOCK : (b + 1) * BLOCK]

    ending = [
        jnp.exp(
            per_block(
                lambda b: totals[0][b] - rows_of(within[0], b) + between(0, b + 1, blocks)
            )
        ),
        jnp.exp(per_block(lambda b: totals[1][b] - rows_of(within[1], b) + between(1, 0, b))),
    ]
    for z in range(2):
        ended = (keys * ending[z]).astype(BF16)
        for g in range(heads):
            st_own[z, g] = dot_tn(
                values[:, g * dv : (g + 1) * dv], ended[:, g * DK : (g + 1) * DK]
            ).astype(BF16)

    def total_copy(z, k):
        to = s + k if z == 0 else s - k
        return pltpu.make_async_remote_copy(
            src_ref=tot_own,
            dst_ref=tot_all.at[z, k],
            send_sem=st_s.at[1, z, k],
            recv_sem=st_r.at[1, z, k],
            device_id={"sp": to},
            device_id_type=MESH,
        )

    def state_pair(z, k):
        to = s + k if z == 0 else s - k
        a = pltpu.make_async_remote_copy(
            src_ref=st_own.at[z],
            dst_ref=st_all.at[z, k],
            send_sem=st_s.at[0, z, k],
            recv_sem=st_r.at[0, z, k],
            device_id={"sp": to},
            device_id_type=MESH,
        )
        return a, total_copy(z, k)

    for k in range(1, n_sp):
        for z in range(2):

            @pl.when(s + k < n_sp if z == 0 else s - k >= 0)
            def _():
                for copy in state_pair(z, k):
                    copy.start()

    for copy in local[5:7]:
        copy.wait()
    acc_q[...] = dot(hid[s, 0:length], whole(wq, s))
    for j in range(1, n_sp):
        relay(2, j)
        multiply(2, j, acc_q, length)
    queries = acc_q[...].astype(BF16).astype(F32)

    tri_row = lax.broadcasted_iota(jnp.int32, (BLOCK, BLOCK), 0)
    tri_col = lax.broadcasted_iota(jnp.int32, (BLOCK, BLOCK), 1)
    masks = [tri_col <= tri_row, tri_col >= tri_row]
    query_dec = [(queries * jnp.exp(within[z])).astype(BF16) for z in range(2)]
    key_dec = [(keys * jnp.exp(-within[z])).astype(BF16) for z in range(2)]
    near = [
        keys * jnp.exp(per_block(lambda b: totals[z][b] - rows_of(within[z], b)))
        for z in range(2)
    ]
    lifted = [
        (queries * jnp.exp(within[0] + per_block(lambda b: between(0, 0, b) + jnp.zeros((BLOCK, 1), F32)))).astype(BF16),
        (queries * jnp.exp(within[1] + per_block(lambda b: between(1, b + 1, blocks) + jnp.zeros((BLOCK, 1), F32)))).astype(BF16),
    ]
    local_out = []
    for g in range(heads):
        cs = slice(g * DK, (g + 1) * DK)
        score_rows = []
        for i in range(blocks):
            line = []
            for j in range(blocks):
                if i == j:
                    score = 0.0
                    for z in range(2):
                        inner = dot_nt(
                            rows_of(query_dec[z], i)[:, cs], rows_of(key_dec[z], j)[:, cs]
                        )
                        score = score + jnp.where(masks[z], inner, 0.0)
                else:
                    z = 0 if j < i else 1
                    gap = between(z, min(i, j) + 1, max(i, j))
                    far = (rows_of(near[z], j) * jnp.exp(gap)).astype(BF16)
                    score = dot_nt(rows_of(query_dec[z], i)[:, cs], far[:, cs])
                line.append(score)
            score_rows.append(jnp.concatenate(line, axis=1))
        scores = jnp.concatenate(score_rows, axis=0).astype(BF16)
        local_out.append(dot(scores, values[:, g * dv : (g + 1) * dv]))

    for k in range(1, n_sp):
        ctx_arrival(1, c_key, k).wait_recv()
        ctx_arrival(2, c_val, k).wait_recv()
    ckeys = jnp.concatenate([c_key[o] for o in range(n_sp)], axis=0).astype(F32)
    cvals = jnp.concatenate([c_val[o] for o in range(n_sp)], axis=0)
    for z in range(2):
        ended = (ckeys * ctx_weight[z]).astype(BF16)
        for g in range(heads):
            fold[z, g] = CTX_LIFT * dot_tn(
                cvals[:, g * dv : (g + 1) * dv], ended[:, g * DK : (g + 1) * DK]
            )

    for k in range(n_sp - 1, 0, -1):
        for z in range(2):

            @pl.when(s - k >= 0 if z == 0 else s + k < n_sp)
            def _():
                for copy in state_pair(z, k):
                    copy.wait_recv()
                decay = jnp.exp(tot_all[z, k][z : z + 1])
                for g in range(heads):
                    fold[z, g] = (
                        fold[z, g] * decay[:, g * DK : (g + 1) * DK]
                        + st_all[z, k, g].astype(F32)
                    )

    for g in range(heads):
        mixed = local_out[g]
        for z in range(2):
            mixed = mixed + dot_nt(
                lifted[z][:, g * DK : (g + 1) * DK], fold[z, g].astype(BF16)
            )
        scale = lax.rsqrt(jnp.mean(mixed * mixed, axis=-1, keepdims=True) + EPS)
        normed[:, g * dv : (g + 1) * dv] = (mixed * scale * head_gain[...]).astype(BF16)

    local[7].wait()
    chunks = rs_s.shape[1]
    span = width // chunks
    rs_copies = []
    for c in range(chunks):
        cols = slice(c * span, (c + 1) * span)
        product = dot(normed[...], wo[:, cols]).astype(BF16)
        for i in range(n_tp):
            part[i, :, cols] = product[i * rows : (i + 1) * rows]
        for k in range(1, n_tp):
            to = lax.rem(t + k, n_tp)
            copy = pltpu.make_async_remote_copy(
                src_ref=part.at[to, :, pl.ds(c * span, span)],
                dst_ref=rs.at[k, :, pl.ds(c * span, span)],
                send_sem=rs_s.at[k, c],
                recv_sem=rs_r.at[k, c],
                device_id={"tp": to},
                device_id_type=MESH,
            )
            copy.start()
            rs_copies.append(copy)
    for c in range(chunks):
        cols = slice(c * span, (c + 1) * span)
        summed = part[t, :, cols].astype(F32)
        for k in range(1, n_tp):
            rs_copies[c * (n_tp - 1) + k - 1].wait_recv()
            summed = summed + rs[k, :, cols].astype(F32)
        projected = summed.astype(BF16).astype(F32)
        out[:, cols] = (latents[:, cols].astype(F32) + gate[:, cols] * projected).astype(BF16)

    for copy in rs_copies + lat_copies + mod_copies:
        copy.wait_send()
    for k in range(1, n_sp):
        for i, buffer in enumerate((c_low, c_key, c_val)):
            ctx_copy(i, buffer, k).wait_send()
        for z in range(2):

            @pl.when(s + k < n_sp if z == 0 else s - k >= 0)
            def _():
                for copy in state_pair(z, k):
                    copy.wait_send()

    for m in range(3):
        for r in range(2):

            @pl.when(onward(r))
            def _():
                ring_copy(m, r, 0, True).wait_send()

            for j in range(1, n_sp):

                @pl.when(exists(r, j))
                def _():
                    mate_copy(m, r, j, h).wait_send()
                    if j < n_sp - 1:

                        @pl.when(onward(r))
                        def _():
                            ring_copy(m, r, j).wait_send()


def per_device(n_sp, n_tp, *args):
    (latents, sv, context, cv, gain, modulator, wq, wk, wv, down, up, bias, extra, hg, wo) = args
    rows, width = latents.shape
    ctx_rows = context.shape[0]
    n_dev = n_sp * n_tp
    length = rows * n_tp
    total = length + ctx_rows
    depth = wq.shape[0]
    kw, vw = wk.shape[1], wv.shape[1]
    heads = bias.shape[1] // DK
    dv = hg.shape[0]
    chunks = 4
    vmem = pl.BlockSpec(memory_space=pltpu.VMEM)
    hbm = pl.BlockSpec(memory_space=pl.ANY)
    dma = pltpu.SemaphoreType.DMA
    scratch = [
        pltpu.VMEM(modulator.shape, BF16),
        pltpu.VMEM((n_dev, 8, modulator.shape[1]), F32),
        pltpu.VMEM((n_tp, rows, width), BF16),
        pltpu.VMEM((n_sp, total, depth), BF16),
        pltpu.VMEM((n_sp, 2, depth // 2, kw), BF16),
        pltpu.VMEM((n_sp, 2, depth // 2, vw), BF16),
        pltpu.VMEM((n_sp, 2, depth // 2, kw), BF16),
        pltpu.VMEM(wo.shape, BF16),
        pltpu.VMEM((total, kw), F32),
        pltpu.VMEM((total, vw), F32),
        pltpu.VMEM((length, kw), F32),
        pltpu.VMEM((n_sp, ctx_rows, down.shape[1]), BF16),
        pltpu.VMEM((n_sp, ctx_rows, kw), BF16),
        pltpu.VMEM((n_sp, ctx_rows, vw), BF16),
        pltpu.VMEM((2, heads, dv, DK), BF16),
        pltpu.VMEM((2, n_sp, heads, dv, DK), BF16),
        pltpu.VMEM((8, kw), F32),
        pltpu.VMEM((2, n_sp, 8, kw), F32),
        pltpu.VMEM((2, heads, dv, DK), F32),
        pltpu.VMEM((length, vw), BF16),
        pltpu.VMEM((n_tp, rows, width), BF16),
        pltpu.VMEM((n_tp, rows, width), BF16),
        dma((8,)),
        dma((n_dev,)),
        dma((n_dev,)),
        dma((n_tp,)),
        dma((n_tp,)),
        dma((3, 2, n_sp)),
        dma((3, 2, n_sp)),
        dma((3, 2, n_sp)),
        dma((3, 2, n_sp)),
        dma((3, n_sp)),
        dma((3, n_sp)),
        dma((2, 2, n_sp)),
        dma((2, 2, n_sp)),
        dma((n_tp, chunks)),
        dma((n_tp, chunks)),
    ]
    return pl.pallas_call(
        functools.partial(kernel, n_sp, n_tp),
        out_shape=jax.ShapeDtypeStruct(latents.shape, BF16),
        in_specs=[vmem] * 5 + [hbm] * 4 + [vmem] * 5 + [hbm],
        out_specs=vmem,
        scratch_shapes=scratch,
        compiler_params=pltpu.CompilerParams(
            collective_id=0, has_side_effects=True, vmem_limit_bytes=56 * 1024 * 1024
        ),
    )(
        latents,
        sv,
        context,
        cv,
        gain.reshape(1, -1),
        modulator,
        wq,
        wk,
        wv,
        down,
        up,
        bias,
        extra,
        hg.reshape(1, -1),
        wo,
    )


def solution(mesh):
    placed = (
        P(("dp", "sp", "tp"), None),
        P("dp", None),
        P(("dp", "sp"), None),
        P(),
        P(),
        P(None, ("sp", "tp")),
        P("sp", "tp"),
        P("sp", "tp"),
        P("sp", "tp"),
        P(),
        P(None, None, "tp"),
        P(None, "tp"),
        P(None, ("dp", "sp"), "tp"),
        P(),
        P("tp", None),
    )
    return jax.shard_map(
        functools.partial(per_device, mesh.shape["sp"], mesh.shape["tp"]),
        mesh=mesh,
        in_specs=placed,
        out_specs=P(("dp", "sp", "tp"), None),
        check_vma=False,
    )
```

time: 278 us -> 87.2 us (0.31)
  blocking collectives: 101 us -> 0 us
  Pallas kernels: 0 us -> 82 us
  waiting for transfers between devices: 45.4 us -> 0 us
  other arithmetic: 43.1 us -> 0 us
  local copies, waits for them, and re-layouts: 40.5 us -> 4.99 us
  matrix products: 31 us -> 0 us
  between operations: 13.7 us -> 0.01 us
    all_gather x6 -> x0, blocking collectives: 101 us -> none  [the longest x1 43.3 us: per_device(): modulation = lax.all_gather(local_mods, ('sp', 'tp'), axis=1, tiled=True)]
    pallas_call x0 -> x1, Pallas kernels: none -> 82 us  [per_device(): pl.pallas_call(functools.partial(kernel, n_sp, n_tp), out_shape=jax.Shape...]
    dot_general x22 -> x0, matrix products: 31 us -> none  [the longest x4 9.18 us: local_sweep(): jnp.einsum('nshd,nshe->nhde', key_blocks * jnp.exp(block_total[:, None] -...]
    reduce_scatter x1 -> x0, waiting for transfers between devices: 24.6 us -> none  [per_device(): lax.psum_scatter(jnp.dot(normed, out_weight, preferred_element_type=jnp.f...]
    all_gather x4 -> x0, waiting for transfers between devices: 18.7 us -> none  [the longest x1 18.7 us: per_device(): lax.all_gather(jnp.stack([forward_state, backward_state])[None].astype(jn...]
    add x13 -> x0, other arithmetic: 13.2 us -> none  [the longest x12 12.9 us: advance(): return (jnp.exp(step_decay)[:, :, None] * carried + step_update, carried)]
    rev x9 -> x0, local copies, waits for them, and re-layouts: 12.9 us -> none  [the longest x1 4.74 us: per_device(): context_value_rows[::-1]]
    another operation x10 -> x0, local copies, waits for them, and re-layouts: 8.28 us -> none  [the longest x6 6.45 us: to_blocks(): return values.reshape((block_count, BLOCK) + values.shape[1:])]
  transfers between devices with their start and end apart: 5 -> 0, of which waited for: 2 -> 0; matrix products, arithmetic and copies ran while one was open for 19% -> 0% of each run, Pallas kernels for 0% -> 0%
where the time goes in v1:
time: 87.2 us; the launch traced here: 87 us
  Pallas kernels  82 us (94%)
  local copies, waits for them, and re-layouts  4.99 us (6%)
    pallas_call x1, Pallas kernels, per_device(): pl.pallas_call(functools.partial(kernel, n_sp, n_tp), out_shape=jax.Shape...  82 us
    unnamed x3, local copies, waits for them, and re-layouts  4.99 us

profile of v1, /device:TPU:0, one launch (start us, length us, event | category | flops | bytes accessed | tf_op | source)
XLA Modules:
  0.0 87.0 jit_solution(6011659150314335607)
XLA Ops:
  0.0 1.5 %copy.17.decay_extra = f32[2,128,2]{2,1,0:T(8,128)} copy(f32[2,128,2]{1,2,0:T(2,128)} %param.27) | data formatting | bytes 4096 | tf_op args[12]
  1.5 1.9 %copy.16.decay_down = bf16[2048,64]{1,0:T(8,128)(2,1)} copy(bf16[2048,64]{0,1:T(8,128)(2,1)} %param.24) | data formatting | bytes 524288 | tf_op args[9]
  3.4 82.0 %shard_map.145 = bf16[32,2048]{1,0:T(8,128)(2,1)} custom-call(bf16[32,2048]{1,0:T(8,128)(2,1)} %latents.1, f32[1,2048]{1,0:T(1,128)} %sample_vector.1, bf16[64,2048]{1,0:T(8,128)(2,1)} %context.1, f32[1,2048]{1,0:T(1,128)} %context_vector.1, f32[1,2048]{1,0:T(1,128)} %bitcast.2, bf16[2048,384]{1,0:T(8,128)(2,1)} %modulator.1, bf16[512,256]{1,0:T(8,128)(2,1)} %query_weight.1, ...), custom_call_target="tpu_custom_call" | custom-call | tf_op jit(solution)/shard_map/pallas_call | solution.py:636
  85.5 1.6 %copy.19 = bf16[32,2048]{1,0:T(8,128)(2,1)} copy(bf16[32,2048]{1,0:T(8,128)(2,1)} %shard_map.145) | data formatting | bytes 262144

commit v2 on v1

--- a/solution.py
+++ b/solution.py
@@ -41,22 +41,32 @@
 def kernel(
     n_sp,
     n_tp,
+    latents_in,
+    sample_vector_in,
+    context_in,
+    context_vector_in,
+    norm_gain_in,
+    modulator,
+    query_weight,
+    key_weight,
+    value_weight,
+    decay_down_in,
+    decay_up_in,
+    decay_bias_in,
+    decay_extra_in,
+    head_gain_in,
+    out_weight,
+    out,
     latents,
     sample_vector,
     context,
     context_vector,
     norm_gain,
-    modulator,
-    query_weight,
-    key_weight,
-    value_weight,
     decay_down,
     decay_up,
     decay_bias,
     decay_extra,
     head_gain,
-    out_weight,
-    out,
     mod_w,
     mods,
     lat,
@@ -68,14 +78,10 @@
     acc_k,
     acc_v,
     acc_q,
-    c_low,
-    c_key,
-    c_val,
+    cbuf,
     st_own,
-    st_all,
-    tot_own,
-    tot_all,
-    fold,
+    st_in,
+    st_out,
     normed,
     part,
     rs,
@@ -88,8 +94,10 @@
     w_r,
     p_s,
     p_r,
-    cx_s,
-    cx_r,
+    cz_s,
+    cz_r,
+    ct_s,
+    ct_r,
     st_s,
     st_r,
     rs_s,
@@ -105,7 +113,8 @@
     rows, width = latents.shape
     ctx_rows = context.shape[0]
     length = rows * n_tp
-    total = length + ctx_rows
+    total = hid.shape[1]
+    ctx_all = n_sp * ctx_rows
     depth = hid.shape[2]
     half = depth // 2
     heads = decay_bias.shape[1] // DK
@@ -126,13 +135,31 @@
                 )
             )
     local.append(pltpu.make_async_copy(out_weight, wo, loc_sem.at[7]))
-    for copy in local:
-        copy.start()
-
     barrier = pltpu.get_barrier_semaphore()
     for k in range(1, n_dev):
         pl.semaphore_signal(barrier, inc=1, device_id=peer(k), device_id_type=MESH)
     pl.semaphore_signal(barrier, inc=1, device_id={"dp": mate}, device_id_type=MESH)
+    small = [
+        pltpu.make_async_copy(source, target, loc_sem.at[8 + i])
+        for i, (source, target) in enumerate(
+            (
+                (sample_vector_in, sample_vector),
+                (context_vector_in, context_vector),
+                (latents_in, latents),
+                (context_in, context),
+                (norm_gain_in, norm_gain),
+                (decay_down_in, decay_down),
+                (decay_up_in, decay_up),
+                (decay_bias_in, decay_bias),
+                (decay_extra_in, decay_extra),
+                (head_gain_in, head_gain),
+            )
+        )
+    ]
+    for copy in small[:4] + local[:1] + small[4:] + local[1:]:
+        copy.start()
+    small[2].wait()
+    small[3].wait()
     pl.semaphore_wait(barrier, n_dev)
 
     def ring_copy(m, r, j, first=False):
@@ -225,16 +252,61 @@
                 device_id_type=MESH,
             )
         )
+    span_t = width // n_tp
+
+    def ctx_line(k):
+        return pltpu.make_async_remote_copy(
+            src_ref=context.at[:, pl.ds(t * span_t, span_t)],
+            dst_ref=cbuf.at[s, :, pl.ds(t * span_t, span_t)],
+            send_sem=cz_s.at[k],
+            recv_sem=cz_r.at[k],
+            device_id={"sp": lax.rem(s + k, n_sp)},
+            device_id_type=MESH,
+        )
+
+    def ctx_line_arrival(k):
+        return pltpu.make_async_remote_copy(
+            src_ref=context.at[:, pl.ds(t * span_t, span_t)],
+            dst_ref=cbuf.at[lax.rem(s - k + n_sp, n_sp), :, pl.ds(t * span_t, span_t)],
+            send_sem=cz_s.at[k],
+            recv_sem=cz_r.at[k],
+            device_id={"sp": s},
+            device_id_type=MESH,
+        )
+
+    def ctx_plane(k, u, owner):
+        view = cbuf.at[lax.rem(s - k + n_sp, n_sp), :, pl.ds(owner * span_t, span_t)]
+        return pltpu.make_async_remote_copy(
+            src_ref=view,
+            dst_ref=view,
+            send_sem=ct_s.at[k, u],
+            recv_sem=ct_r.at[k, u],
+            device_id={"tp": lax.rem(t + u, n_tp)},
+            device_id_type=MESH,
+        )
+
+    for k in range(1, n_sp):
+        ctx_line(k).start()
+    for copy in lat_copies:
+        copy.start()
     send_own(0)
     send_own(1)
-    for copy in lat_copies:
-        copy.start()
-
+    queue = [(m, j) for j in range(1, n_sp) for m in range(2)]
+
+    def relay_next():
+        if queue:
+            m, j = queue.pop(0)
+            relay(m, j)
+            if (m, j) == (1, max(n_sp - 2, 1)):
+                send_own(2)
+
+    small[0].wait()
+    small[1].wait()
     is_first = lax.broadcasted_iota(jnp.int32, (16, width), 0) == 0
     vectors = jnp.where(is_first, sample_vector[...], context_vector[...])
     conditions = (vectors / (1.0 + jnp.exp(-vectors))).astype(BF16)
     local[0].wait()
-    mods[me] = dot(conditions, mod_w[...])[0:8]
+    mods[me] = dot(conditions, mod_w[...])[0:2]
     mod_copies = []
     for k in range(1, n_dev):
         copy = pltpu.make_async_remote_copy(
@@ -248,7 +320,13 @@
         copy.start()
         mod_copies.append(copy)
 
+    for k in range(1, n_sp):
+        ctx_line_arrival(k).wait_recv()
+        for u in range(1, n_tp):
+            ctx_plane(k, u, t).start()
+    relay_next()
     lat[t] = latents[...]
+    cbuf[s] = context[...]
     for k in range(1, n_tp):
         pltpu.make_async_remote_copy(
             src_ref=latents,
@@ -268,6 +346,8 @@
             device_id={"tp": t},
             device_id_type=MESH,
         ).wait_recv()
+    for copy in small[4:]:
+        copy.wait()
     modulation = jnp.concatenate([mods[i] for i in range(n_dev)], axis=1)
     gate = modulation[0:1, 2 * width :]
 
@@ -285,58 +365,42 @@
 
     for i in range(n_tp):
         put(modulated(lat[i], 0), i * rows)
+    relay_next()
+    for k in range(1, n_sp):
+        for u in range(1, n_tp):
+            ctx_plane(k, u, lax.rem(t - u + n_tp, n_tp)).wait_recv()
     piece = min(32, ctx_rows)
-    for i in range(ctx_rows // piece):
-        put(modulated(context[i * piece : (i + 1) * piece], 1), length + i * piece)
-
-    low = dot(hid[0], decay_down[0:depth])
+    for o in range(n_sp):
+        for i in range(ctx_rows // piece):
+            put(
+                modulated(cbuf[o, i * piece : (i + 1) * piece], 1),
+                length + o * ctx_rows + i * piece,
+            )
+
+    low = dot_nt(hid[0], decay_down[:, 0:depth])
     for o in range(1, n_sp):
-        low = low + dot(hid[o], decay_down[o * depth : (o + 1) * depth])
+        low = low + dot_nt(hid[o], decay_down[:, o * depth : (o + 1) * depth])
     low = low.astype(BF16)
 
-    def ctx_copy(i, buffer, k):
-        other = lax.rem(s + k, n_sp)
-        return pltpu.make_async_remote_copy(
-            src_ref=buffer.at[s],
-            dst_ref=buffer.at[s],
-            send_sem=cx_s.at[i, k],
-            recv_sem=cx_r.at[i, k],
-            device_id={"sp": other},
-            device_id_type=MESH,
-        )
-
-    def ctx_arrival(i, buffer, k):
-        other = lax.rem(s - k + n_sp, n_sp)
-        return pltpu.make_async_remote_copy(
-            src_ref=buffer.at[s],
-            dst_ref=buffer.at[other],
-            send_sem=cx_s.at[i, k],
-            recv_sem=cx_r.at[i, k],
-            device_id={"sp": s},
-            device_id_type=MESH,
-        )
-
-    c_low[s] = low[length:]
-    for k in range(1, n_sp):
-        ctx_copy(0, c_low, k).start()
+    relay_next()
 
     def log_decays(values, z):
         x = dot(values[:, z * rank : (z + 1) * rank], decay_up[z]) + decay_bias[z : z + 1]
         return log_sigmoid(x) / SHARP
 
-    def wide(z):
-        extra = decay_extra[z]
-        return jnp.concatenate(
-            [jnp.broadcast_to(extra[:, g : g + 1], (length, DK)) for g in range(heads)], axis=1
-        )
-
     row_id = lax.broadcasted_iota(jnp.int32, (length, length), 0)
     col_id = lax.broadcasted_iota(jnp.int32, (length, length), 1)
     same = row_id // BLOCK == col_id // BLOCK
-    within = [
-        sums(same & (col_id <= row_id), log_decays(low[:length], 0) + wide(0)),
-        sums(same & (col_id >= row_id), log_decays(low[:length], 1) + wide(1)),
-    ]
+    inner = [same & (col_id <= row_id), same & (col_id >= row_id)]
+
+    def extra_sums(z):
+        columns = [
+            jnp.sum(jnp.where(inner[z], decay_extra[z, g : g + 1, :], 0.0), axis=1, keepdims=True)
+            for g in range(heads)
+        ]
+        return jnp.concatenate([jnp.broadcast_to(c, (length, DK)) for c in columns], axis=1)
+
+    within = [sums(inner[z], log_decays(low[:length], z)) + extra_sums(z) for z in range(2)]
     blocks = length // BLOCK
     totals = [
         [within[0][(b + 1) * BLOCK - 1 : (b + 1) * BLOCK] for b in range(blocks)],
@@ -350,14 +414,7 @@
             value = value + totals[z][b]
         return value
 
-    tot_own[...] = jnp.concatenate(
-        [between(0, 0, blocks), between(1, 0, blocks)] + [none] * 6, axis=0
-    )
-
-    for k in range(1, n_sp):
-        ctx_arrival(0, c_low, k).wait_recv()
-    lows = jnp.concatenate([c_low[o] for o in range(n_sp)], axis=0)
-    ctx_all = n_sp * ctx_rows
+    lows = low[length:]
     crow = lax.broadcasted_iota(jnp.int32, (ctx_all, ctx_all), 0)
     ccol = lax.broadcasted_iota(jnp.int32, (ctx_all, ctx_all), 1)
     ctx_weight = [
@@ -369,20 +426,18 @@
         copy.wait()
     acc_k[...] = dot(hid[s], whole(wk, s))
     acc_v[...] = dot(hid[s], whole(wv, s))
-    for j in range(1, n_sp):
-        relay(0, j)
-        relay(1, j)
-        if j == n_sp - 1:
-            send_own(2)
+    multiply(0, 1, acc_k, total)
+    relay_next()
+    multiply(1, 1, acc_v, total)
+    for j in range(2, n_sp):
+        relay_next()
         multiply(0, j, acc_k, total)
+        relay_next()
         multiply(1, j, acc_v, total)
     keys = acc_k[...].astype(BF16)
     values = acc_v[...].astype(BF16)
-    c_key[s] = keys[length:]
-    c_val[s] = values[length:]
-    for k in range(1, n_sp):
-        ctx_copy(1, c_key, k).start()
-        ctx_copy(2, c_val, k).start()
+    ckeys = keys[length:].astype(F32)
+    cvals = values[length:]
     keys = keys[:length].astype(F32)
     values = values[:length]
 
@@ -405,45 +460,66 @@
         for g in range(heads):
             st_own[z, g] = dot_tn(
                 values[:, g * dv : (g + 1) * dv], ended[:, g * DK : (g + 1) * DK]
-            ).astype(BF16)
-
-    def total_copy(z, k):
-        to = s + k if z == 0 else s - k
+            )
+
+    def begins(z):
+        return s == 0 if z == 0 else s == n_sp - 1
+
+    def goes_on(z):
+        return s < n_sp - 1 if z == 0 else s > 0
+
+    def state_copy(z, g):
         return pltpu.make_async_remote_copy(
-            src_ref=tot_own,
-            dst_ref=tot_all.at[z, k],
-            send_sem=st_s.at[1, z, k],
-            recv_sem=st_r.at[1, z, k],
-            device_id={"sp": to},
-            device_id_type=MESH,
-        )
-
-    def state_pair(z, k):
-        to = s + k if z == 0 else s - k
-        a = pltpu.make_async_remote_copy(
-            src_ref=st_own.at[z],
-            dst_ref=st_all.at[z, k],
-            send_sem=st_s.at[0, z, k],
-            recv_sem=st_r.at[0, z, k],
-            device_id={"sp": to},
-            device_id_type=MESH,
-        )
-        return a, total_copy(z, k)
-
-    for k in range(1, n_sp):
+            src_ref=st_out.at[z, g],
+            dst_ref=st_in.at[z, g],
+            send_sem=st_s.at[z, g],
+            recv_sem=st_r.at[z, g],
+            device_id={"sp": s + 1 if z == 0 else s - 1},
+            device_id_type=MESH,
+        )
+
+    whole_decay = [jnp.exp(between(z, 0, blocks)) for z in range(2)]
+
+    def pass_on(z, g):
+        @pl.when(goes_on(z))
+        def _():
+            decay = whole_decay[z][:, g * DK : (g + 1) * DK]
+            st_out[z, g] = (st_in[z, g].astype(F32) * decay + st_own[z, g]).astype(BF16)
+            state_copy(z, g).start()
+
+    for z in range(2):
+
+        @pl.when(begins(z))
+        def _():
+            ended = (ckeys * ctx_weight[z]).astype(BF16)
+            for g in range(heads):
+                st_in[z, g] = (
+                    CTX_LIFT
+                    * dot_tn(cvals[:, g * dv : (g + 1) * dv], ended[:, g * DK : (g + 1) * DK])
+                ).astype(BF16)
+                pass_on(z, g)
+
+    def chain(near):
         for z in range(2):
-
-            @pl.when(s + k < n_sp if z == 0 else s - k >= 0)
+            ahead = 2 * s < n_sp - 1 if z == 0 else 2 * s >= n_sp - 1
+            turn = ahead if near else jnp.logical_not(ahead)
+
+            @pl.when(jnp.logical_and(turn, jnp.logical_not(begins(z))))
             def _():
-                for copy in state_pair(z, k):
-                    copy.start()
+                for g in range(heads):
+                    state_copy(z, g).wait_recv()
+                    pass_on(z, g)
 
     for copy in local[5:7]:
         copy.wait()
     acc_q[...] = dot(hid[s, 0:length], whole(wq, s))
     for j in range(1, n_sp):
         relay(2, j)
+        if j == 1:
+            chain(True)
         multiply(2, j, acc_q, length)
+        if j == max(n_sp - 2, 1):
+            chain(False)
     queries = acc_q[...].astype(BF16).astype(F32)
 
     tri_row = lax.broadcasted_iota(jnp.int32, (BLOCK, BLOCK), 0)
@@ -483,37 +559,11 @@
         scores = jnp.concatenate(score_rows, axis=0).astype(BF16)
         local_out.append(dot(scores, values[:, g * dv : (g + 1) * dv]))
 
-    for k in range(1, n_sp):
-        ctx_arrival(1, c_key, k).wait_recv()
-        ctx_arrival(2, c_val, k).wait_recv()
-    ckeys = jnp.concatenate([c_key[o] for o in range(n_sp)], axis=0).astype(F32)
-    cvals = jnp.concatenate([c_val[o] for o in range(n_sp)], axis=0)
-    for z in range(2):
-        ended = (ckeys * ctx_weight[z]).astype(BF16)
-        for g in range(heads):
-            fold[z, g] = CTX_LIFT * dot_tn(
-                cvals[:, g * dv : (g + 1) * dv], ended[:, g * DK : (g + 1) * DK]
-            )
-
-    for k in range(n_sp - 1, 0, -1):
-        for z in range(2):
-
-            @pl.when(s - k >= 0 if z == 0 else s + k < n_sp)
-            def _():
-                for copy in state_pair(z, k):
-                    copy.wait_recv()
-                decay = jnp.exp(tot_all[z, k][z : z + 1])
-                for g in range(heads):
-                    fold[z, g] = (
-                        fold[z, g] * decay[:, g * DK : (g + 1) * DK]
-                        + st_all[z, k, g].astype(F32)
-                    )
-
     for g in range(heads):
         mixed = local_out[g]
         for z in range(2):
             mixed = mixed + dot_nt(
-                lifted[z][:, g * DK : (g + 1) * DK], fold[z, g].astype(BF16)
+                lifted[z][:, g * DK : (g + 1) * DK], st_in[z, g]
             )
         scale = lax.rsqrt(jnp.mean(mixed * mixed, axis=-1, keepdims=True) + EPS)
         normed[:, g * dv : (g + 1) * dv] = (mixed * scale * head_gain[...]).astype(BF16)
@@ -551,14 +601,15 @@
     for copy in rs_copies + lat_copies + mod_copies:
         copy.wait_send()
     for k in range(1, n_sp):
-        for i, buffer in enumerate((c_low, c_key, c_val)):
-            ctx_copy(i, buffer, k).wait_send()
-        for z in range(2):
-
-            @pl.when(s + k < n_sp if z == 0 else s - k >= 0)
-            def _():
-                for copy in state_pair(z, k):
-                    copy.wait_send()
+        ctx_line(k).wait_send()
+        for u in range(1, n_tp):
+            ctx_plane(k, u, t).wait_send()
+    for z in range(2):
+
+        @pl.when(goes_on(z))
+        def _():
+            for g in range(heads):
+                state_copy(z, g).wait_send()
 
     for m in range(3):
         for r in range(2):
@@ -585,7 +636,7 @@
     ctx_rows = context.shape[0]
     n_dev = n_sp * n_tp
     length = rows * n_tp
-    total = length + ctx_rows
+    total = length + n_sp * ctx_rows
     depth = wq.shape[0]
     kw, vw = wk.shape[1], wv.shape[1]
     heads = bias.shape[1] // DK
@@ -595,8 +646,18 @@
     hbm = pl.BlockSpec(memory_space=pl.ANY)
     dma = pltpu.SemaphoreType.DMA
     scratch = [
+        pltpu.VMEM(latents.shape, BF16),
+        pltpu.VMEM(sv.shape, F32),
+        pltpu.VMEM(context.shape, BF16),
+        pltpu.VMEM(cv.shape, F32),
+        pltpu.VMEM((1, width), F32),
+        pltpu.VMEM(down.shape[::-1], BF16),
+        pltpu.VMEM(up.shape, BF16),
+        pltpu.VMEM(bias.shape, F32),
+        pltpu.VMEM((2, heads, length), F32),
+        pltpu.VMEM((1, dv), F32),
         pltpu.VMEM(modulator.shape, BF16),
-        pltpu.VMEM((n_dev, 8, modulator.shape[1]), F32),
+        pltpu.VMEM((n_dev, 2, modulator.shape[1]), F32),
         pltpu.VMEM((n_tp, rows, width), BF16),
         pltpu.VMEM((n_sp, total, depth), BF16),
         pltpu.VMEM((n_sp, 2, depth // 2, kw), BF16),
@@ -606,18 +667,14 @@
         pltpu.VMEM((total, kw), F32),
         pltpu.VMEM((total, vw), F32),
         pltpu.VMEM((length, kw), F32),
-        pltpu.VMEM((n_sp, ctx_rows, down.shape[1]), BF16),
-        pltpu.VMEM((n_sp, ctx_rows, kw), BF16),
-        pltpu.VMEM((n_sp, ctx_rows, vw), BF16),
+        pltpu.VMEM((n_sp, ctx_rows, width), BF16),
+        pltpu.VMEM((2, heads, dv, DK), F32),
         pltpu.VMEM((2, heads, dv, DK), BF16),
-        pltpu.VMEM((2, n_sp, heads, dv, DK), BF16),
-        pltpu.VMEM((8, kw), F32),
-        pltpu.VMEM((2, n_sp, 8, kw), F32),
-        pltpu.VMEM((2, heads, dv, DK), F32),
+        pltpu.VMEM((2, heads, dv, DK), BF16),
         pltpu.VMEM((length, vw), BF16),
         pltpu.VMEM((n_tp, rows, width), BF16),
         pltpu.VMEM((n_tp, rows, width), BF16),
-        dma((8,)),
+        dma((18,)),
         dma((n_dev,)),
         dma((n_dev,)),
         dma((n_tp,)),
@@ -626,17 +683,19 @@
         dma((3, 2, n_sp)),
         dma((3, 2, n_sp)),
         dma((3, 2, n_sp)),
-        dma((3, n_sp)),
-        dma((3, n_sp)),
-        dma((2, 2, n_sp)),
-        dma((2, 2, n_sp)),
+        dma((n_sp,)),
+        dma((n_sp,)),
+        dma((n_sp, n_tp)),
+        dma((n_sp, n_tp)),
+        dma((2, heads)),
+        dma((2, heads)),
         dma((n_tp, chunks)),
         dma((n_tp, chunks)),
     ]
     return pl.pallas_call(
         functools.partial(kernel, n_sp, n_tp),
         out_shape=jax.ShapeDtypeStruct(latents.shape, BF16),
-        in_specs=[vmem] * 5 + [hbm] * 4 + [vmem] * 5 + [hbm],
+        in_specs=[hbm] * 15,
         out_specs=vmem,
         scratch_shapes=scratch,
         compiler_params=pltpu.CompilerParams(
@@ -652,10 +711,10 @@
         wq,
         wk,
         wv,
-        down,
+        down.T,
         up,
         bias,
-        extra,
+        extra.transpose(0, 2, 1),
         hg.reshape(1, -1),
         wo,
     )

time: 87.2 us -> 68.9 us (0.79)
  Pallas kernels: 82 us -> 67.2 us
  local copies, waits for them, and re-layouts: 4.99 us -> 1.57 us
    pallas_call x1, Pallas kernels: 82 us -> 67.2 us  [per_device(): pl.pallas_call(functools.partial(kernel, n_sp, n_tp), out_shape=jax.Shape...]
    unnamed x3 -> x1, local copies, waits for them, and re-layouts: 4.99 us -> 1.57 us
where the time goes in v2:
time: 68.9 us; the launch traced here: 68.8 us
  Pallas kernels  67.2 us (98%)
  local copies, waits for them, and re-layouts  1.57 us (2%)
    pallas_call x1, Pallas kernels, per_device(): pl.pallas_call(functools.partial(kernel, n_sp, n_tp), out_shape=jax.Shape...  67.2 us
    unnamed x1, local copies, waits for them, and re-layouts  1.57 us

profile of v2, /device:TPU:0, one launch (start us, length us, event | category | flops | bytes accessed | tf_op | source)
XLA Modules:
  0.0 68.8 jit_solution(7599263260432708348)
XLA Ops:
  0.0 67.2 %shard_map.145 = bf16[32,2048]{1,0:T(8,128)(2,1)} custom-call(bf16[32,2048]{1,0:T(8,128)(2,1)} %latents_in.1, f32[1,2048]{1,0:T(1,128)} %sample_vector_in.1, bf16[64,2048]{1,0:T(8,128)(2,1)} %context_in.1, f32[1,2048]{1,0:T(1,128)} %context_vector_in.1, f32[1,2048]{1,0:T(1,128)} %bitcast.5, bf16[2048,384]{1,0:T(8,128)(2,1)} %modulator.1, ...), custom_call_target="tpu_custom_call" | custom-call | tf_op jit(solution)/shard_map/pallas_call | solution.py:695
  67.2 1.6 %copy.17 = bf16[32,2048]{1,0:T(8,128)(2,1)} copy(bf16[32,2048]{1,0:T(8,128)(2,1)} %shard_map.145) | data formatting | bytes 262144
